TPU v7x, 32 devices: a whole 2x2x4 slice. The times are simulated.
32 devices in a mesh: sp: 8 (over z, y), tp: 4 (over x, core).
Axes of the slice: x: 2, y: 2, z: 4, core: 2. Of those that a mesh axis runs over, the one named last changes fastest.
Arguments:
- resid_in: bfloat16 [2048, 2048], P('sp'), may hold values from -6 to 6
- query_latent: bfloat16 [2048, 768], P('sp'), may hold values from -6 to 6
- kv_latent: bfloat16 [2048, 512], P('sp'), may hold values from -6 to 6
- rotary_key: bfloat16 [2048, 64], P('sp'), may hold values from -200 to 200
- query_gain: float32 [768], replicated, may hold values from 0.1 to 1.9
- kv_gain: float32 [512], replicated, may hold values from 0.1 to 1.9
- w_query_plain: bfloat16 [768, 2048], P(None, 'tp'), may hold values from -0.875 to 0.875
- w_query_rotary: bfloat16 [768, 1024], P(None, 'tp'), may hold values from -0.875 to 0.875
- w_key_plain: bfloat16 [512, 2048], P(None, 'tp'), may hold values from -0.25 to 0.25
- w_value: bfloat16 [512, 2048], P(None, 'tp'), may hold values from -0.25 to 0.25
- w_output: bfloat16 [2048, 2048], P('tp'), may hold values from -0.125 to 0.125
- ffn_gain: float32 [2048], replicated, may hold values from 0.1 to 1.9
- w_gate: bfloat16 [2048, 5632], P('sp', 'tp'), may hold values from -0.125 to 0.125
- w_up: bfloat16 [2048, 5632], P('sp', 'tp'), may hold values from -0.125 to 0.125
- w_down: bfloat16 [5632, 2048], P('tp', 'sp'), may hold values from -0.078125 to 0.078125
Outputs:
- resid_out: bfloat16 [2048, 2048], P(('sp', 'tp'))
All inputs are finite; a program needn't handle non-finite values.
Results may differ from a plain program's by a relative error of at most 0.014.
The roundings to bfloat16 on the way count: a program that leaves them out, or rounds other values in their place, can miss the bound.
Values may be sent and summed in bfloat16 or wider, within the bound.
No kernel may reach another device: no remote copies, remote signals or barrier semaphores. Data moves between devices by JAX's collectives and lax.ppermute only.
A program may use at most 192 MiB of HBM per device.

v0:
```python
import jax
import jax.numpy as jnp
from jax import lax
from jax.sharding import PartitionSpec as P

NOPE = 128
ROPE = 64
VDIM = 128


def normed(values, gain):
    wide = values.astype(jnp.float32)
    return wide * lax.rsqrt(jnp.mean(wide * wide, axis=-1, keepdims=True) + 1e-06) * gain


def rotate(values, cosine, sine):
    half = values.shape[-1] // 2
    first = values[..., :half]
    second = values[..., half:]
    return jnp.concatenate(
        [first * cosine - second * sine, second * cosine + first * sine], axis=-1
    )


def attend(carry, q_plain, q_rot, k_plain, values, key_rot):
    top, total, acc = carry
    scale = (NOPE + ROPE) ** (-0.5)
    score = (
        jnp.einsum("qhd,khd->hqk", q_plain, k_plain, preferred_element_type=jnp.float32)
        + jnp.einsum("qhr,kr->hqk", q_rot, key_rot, preferred_element_type=jnp.float32)
    ) * scale
    new_top = jnp.maximum(top, jnp.max(score, axis=-1))
    weight = jnp.exp(score - new_top[:, :, None])
    total = jnp.sum(weight, axis=-1)
    mixed = jnp.einsum(
        "hqk,khd->qhd", weight.astype(jnp.bfloat16), values, preferred_element_type=jnp.float32
    )
    acc = mixed
    return (new_top, total, acc)


def shards(
    resid_in,
    query_latent,
    kv_latent,
    rotary_key,
    query_gain,
    kv_gain,
    w_query_plain,
    w_query_rotary,
    w_key_plain,
    w_value,
    w_output,
    ffn_gain,
    w_gate,
    w_up,
    w_down,
):
    tok = resid_in.shape[0]
    heads_dev = w_query_plain.shape[1] // NOPE
    offset = lax.axis_index("sp") * tok
    position = (offset + jnp.arange(tok, dtype=jnp.int32)).astype(jnp.float32)
    freq = 10000.0 ** (-jnp.arange(0, ROPE, 2, dtype=jnp.float32) / ROPE)
    angle = position[:, None] * freq[None, :]
    cosine = jnp.cos(angle)
    sine = jnp.sin(angle)
    q_norm = normed(query_latent, query_gain).astype(jnp.bfloat16)
    kv_norm = normed(kv_latent, kv_gain).astype(jnp.bfloat16)
    key_rot = rotate(rotary_key.astype(jnp.float32), cosine, sine).astype(jnp.bfloat16)
    q_plain = (
        jnp.dot(q_norm, w_query_plain, preferred_element_type=jnp.float32)
        .astype(jnp.bfloat16)
        .reshape(tok, heads_dev, NOPE)
    )
    q_raw = jnp.dot(q_norm, w_query_rotary, preferred_element_type=jnp.float32).reshape(
        tok, heads_dev, ROPE
    )
    q_rot = rotate(q_raw, cosine[:, None, :], sine[:, None, :]).astype(jnp.bfloat16)
    start_carry = (
        jnp.full((heads_dev, tok), -1e30, jnp.float32),
        jnp.zeros((heads_dev, tok), jnp.float32),
        jnp.zeros((tok, heads_dev, VDIM), jnp.float32),
    )
    latent = lax.all_gather(kv_norm, "sp", axis=0, tiled=True)
    rot_piece = lax.all_gather(key_rot, "sp", axis=0, tiled=True)
    count = latent.shape[0]
    k_piece = (
        jnp.dot(latent, w_key_plain, preferred_element_type=jnp.float32)
        .astype(jnp.bfloat16)
        .reshape(count, heads_dev, NOPE)
    )
    v_piece = (
        jnp.dot(latent, w_value, preferred_element_type=jnp.float32)
        .astype(jnp.bfloat16)
        .reshape(count, heads_dev, VDIM)
    )
    top, total, acc = attend(start_carry, q_plain, q_rot, k_piece, v_piece, rot_piece)
    attn = (
        (acc / jnp.transpose(total)[:, :, None]).astype(jnp.bfloat16).reshape(tok, heads_dev * VDIM)
    )
    partial_out = jnp.dot(attn, w_output, preferred_element_type=jnp.float32)
    share = tok // lax.axis_size("tp")
    own_start = lax.axis_index("tp") * share
    mid = resid_in.astype(jnp.float32) + lax.psum(partial_out.astype(jnp.bfloat16), "tp").astype(
        jnp.float32
    )
    h_norm = normed(mid, ffn_gain).astype(jnp.bfloat16)
    mid_own = lax.dynamic_slice_in_dim(mid, own_start, share, 0)
    gate = jnp.dot(
        h_norm, lax.all_gather(w_gate, "sp", axis=0, tiled=True), preferred_element_type=jnp.float32
    )
    upper = jnp.dot(
        h_norm, lax.all_gather(w_up, "sp", axis=0, tiled=True), preferred_element_type=jnp.float32
    )
    hidden = (jax.nn.silu(gate) * upper).astype(jnp.bfloat16)
    terms = jnp.dot(
        hidden, lax.all_gather(w_down, "sp", axis=1, tiled=True), preferred_element_type=jnp.float32
    )
    ffn_own = lax.psum_scatter(
        terms.astype(jnp.bfloat16), "tp", scatter_dimension=0, tiled=True
    ).astype(jnp.float32)
    return (mid_own + ffn_own).astype(jnp.bfloat16)


def solution(mesh):
    return jax.shard_map(
        shards,
        mesh=mesh,
        in_specs=(
            P("sp", None),
            P("sp", None),
            P("sp", None),
            P("sp", None),
            P(),
            P(),
            P(None, "tp"),
            P(None, "tp"),
            P(None, "tp"),
            P(None, "tp"),
            P("tp", None),
            P(),
            P("sp", "tp"),
            P("sp", "tp"),
            P("tp", "sp"),
        ),
        out_specs=P(("sp", "tp"), None),
        check_vma=False,
    )
```

profile of v0, /device:TPU:0, one launch (start us, length us, event | category | flops | bytes accessed | tf_op | source)
XLA Modules:
  0.0 431.7 jit_solution(17128498357206020806)
XLA Ops:
  6.5 0.0 copy-start
  6.5 0.0 all-gather.5.cloned.1.call-start
  6.5 1.2 fusion.20
  7.8 1.8 fusion.22
  9.6 0.0 all-gather.5.cloned.1.call-update
  9.6 0.0 all-reduce.2.cloned.1.call-start
  9.7 0.0 copy-start.4
  9.7 0.8 convert_element_type.71
  10.5 0.2 multiply_cosine_fusion
  10.7 32.9 %all_gather.16 = bf16[2048,64]{0,1:T(8,128)(2,1)S(1)} all-gather(bf16[256,64]{0,1:T(8,128)(2,1)S(1)} %pad_maximum_fusion), channel_id=1, replica_groups=mesh['sp'=8,'tp'=4] {'sp'}, dimensions={0}, use_global_device_ids=true | all-gather | bytes 294912 | tf_op jit(solution)/shard_map/all_gather | solution.py:85
  43.6 1.2 fusion.17
  44.8 0.0 copy-done.2
  44.8 0.0 copy-done.8
  44.8 1.6 fusion.10
  46.4 0.4 fusion.30
  46.9 15.4 %all-gather.5.cloned.1.call-done = bf16[2048,512]{1,0:T(8,128)(2,1)} async-done(((bf16[256,512]{1,0:T(8,128)(2,1)}), bf16[2048,512]{1,0:T(8,128)(2,1)}) %all-gather.5.cloned.1.call-update) | async-done | bytes 2097168 | tf_op jit(solution)/shard_map/all_gather | solution.py:84
  62.3 2.9 convolution_convert_fusion
  65.2 1.2 fusion.23
  66.4 1.4 fusion.36
  67.9 0.0 copy-start.5
  67.9 1.3 fusion.1
  69.2 0.3 copy-done.3
  69.4 0.1 copy-done.5
  69.5 1.3 convolution_convert_fusion.1
  70.9 1.8 fusion.14
  72.6 0.0 copy-done
  72.6 1.7 convolution_convert_fusion.2
  74.4 0.0 all-reduce.2.cloned.1.call-update
  74.4 0.0 all-gather.7.cloned.1.call-start
  74.4 0.7 all-gather.7.cloned.1.call-update
  75.1 0.0 all-gather.11.cloned.1.call-start
  75.2 0.5 all-gather.11.cloned.1.call-update
  75.7 0.0 all-gather.9.cloned.1.call-start
  75.8 0.5 all-gather.9.cloned.1.call-update
  76.3 0.0 copy-start.7
  76.3 0.2 reduce-scatter.2.cloned.1.call-start
  76.5 32.9 %all-reduce.2.cloned.1.call-done = bf16[256,2048]{1,0:T(8,128)(2,1)} async-done(((bf16[256,2048]{1,0:T(8,128)(2,1)}), bf16[256,2048]{1,0:T(8,128)(2,1)}) %all-reduce.2.cloned.1.call-update) | async-done | bytes 1048592 | tf_op jit(solution)/shard_map/psum | solution.py:104
  109.4 0.0 copy-done.1
  109.4 2.9 convert_add_fusion
  112.4 92.1 %all-gather.7.cloned.1.call-done = bf16[2048,1408]{1,0:T(8,128)(2,1)} async-done(((bf16[256,1408]{1,0:T(8,128)(2,1)}), bf16[2048,1408]{1,0:T(8,128)(2,1)}) %all-gather.7.cloned.1.call-update) | async-done | bytes 5767184 | tf_op jit(solution)/shard_map/all_gather | solution.py:110
  204.4 0.0 copy-done.7
  204.5 5.9 %fusion.35 = f32[256,1408]{1,0:T(8,128)} fusion(bf16[2048,1408]{1,0:T(8,128)(2,1)} %all-gather.7.cloned.1.call-done, f32[2048]{0:T(1024)S(1)} %copy-done.7, f32[256]{0:T(256)S(1)} %add_rsqrt_fusion, bf16[256,2048]{1,0:T(8,128)(2,1)} %all-reduce.2.cloned.1.call-done, bf16[256,2048]{1,0:T(8,128)(2,1)S(1)} %copy-done.1), kind=kOutput, calls=%fused_computation.55 | convolution fusion | flops 1479540736 | bytes 9315328 | tf_op jit(solution)/shard_map/dot_general | solution.py:109
  210.4 87.3 %all-gather.11.cloned.1.call-done = bf16[1408,2048]{1,0:T(8,128)(2,1)} async-done(((bf16[1408,256]{1,0:T(8,128)(2,1)}), bf16[1408,2048]{1,0:T(8,128)(2,1)}) %all-gather.11.cloned.1.call-update) | async-done | bytes 5767184 | tf_op jit(solution)/shard_map/all_gather | solution.py:117
  297.7 92.6 %all-gather.9.cloned.1.call-done = bf16[2048,1408]{1,0:T(8,128)(2,1)} async-done(((bf16[256,1408]{1,0:T(8,128)(2,1)}), bf16[2048,1408]{1,0:T(8,128)(2,1)}) %all-gather.9.cloned.1.call-update) | async-done | bytes 5767184 | tf_op jit(solution)/shard_map/all_gather | solution.py:113
  390.2 9.6 %convolution_convert_fusion.3 = bf16[256,2048]{1,0:T(8,128)(2,1)} fusion(bf16[1408,2048]{1,0:T(8,128)(2,1)} %all-gather.11.cloned.1.call-done, bf16[2048,1408]{1,0:T(8,128)(2,1)} %all-gather.9.cloned.1.call-done, f32[256,1408]{1,0:T(8,128)} %fusion.35, f32[2048]{0:T(1024)S(1)} %copy-done.7, f32[256]{0:T(256)S(1)} %add_rsqrt_fusion, ...), kind=kOutput, calls=%fused_computation.12 | convolution fusion | flops 2958622720 | bytes 16131072 | tf_op jit(solution)/shard_map/dot_general | solution.py:116
  399.9 0.0 reduce-scatter.2.cloned.1.call-update
  399.9 23.1 %reduce-scatter.2.cloned.1.call-done = bf16[64,2048]{1,0:T(8,128)(2,1)} async-done(((bf16[256,2048]{1,0:T(8,128)(2,1)}), bf16[64,2048]{1,0:T(8,128)(2,1)}) %reduce-scatter.2.cloned.1.call-update) | async-done | bytes 262160 | tf_op jit(solution)/shard_map/reduce_scatter | solution.py:119
  423.0 1.9 add_convert_fusion
  (15 shorter events, 0.1 us)
Async XLA Ops:
  6.5 66.1 %copy-start = (bf16[512,2048]{1,0:T(8,128)(2,1)S(1)}, bf16[512,2048]{1,0:T(8,128)(2,1)}, u32[]{:S(2)}) copy-start(bf16[512,2048]{1,0:T(8,128)(2,1)} %param.25) | copy-start | bytes 6291460
  6.5 38.3 %copy-start.2 = (bf16[256,768]{1,0:T(8,128)(2,1)S(1)}, bf16[256,768]{1,0:T(8,128)(2,1)}, u32[]{:S(2)}) copy-start(bf16[256,768]{1,0:T(8,128)(2,1)} %param.16) | copy-start | bytes 1179652
  6.5 38.3 %copy-start.8 = (f32[768]{0:T(1024)S(1)}, f32[768]{0:T(1024)}, u32[]{:S(2)}) copy-start(f32[768]{0:T(1024)} %param.19) | copy-start | bytes 9220
  6.5 55.7 %all-gather.5.cloned.1.call-start = ((), (), s32[]{:S(2)}) async-start(), calls=%async_computation.1 | async-start | bytes 2359296 | tf_op jit(solution)/shard_map/all_gather | solution.py:84
  9.6 99.8 %all-reduce.2.cloned.1.call-start = ((), (), s32[]{:S(2)}) async-start(), calls=%async_computation.2 | async-start | bytes 2097152 | tf_op jit(solution)/shard_map/psum | solution.py:104
  9.7 52.6 %copy-start.4 = (bf16[512,512]{1,0:T(8,128)(2,1)S(1)}, bf16[512,512]{1,0:T(8,128)(2,1)}, u32[]{:S(2)}) copy-start(bf16[512,512]{1,0:T(8,128)(2,1)} %param.23) | copy-start | bytes 1572868
  10.5 35.9 %copy-start.6 = (bf16[768,256]{1,0:T(8,128)(2,1)S(1)}, bf16[768,256]{1,0:T(8,128)(2,1)}, u32[]{:S(2)}) copy-start(bf16[768,256]{1,0:T(8,128)(2,1)} %param.22) | copy-start | bytes 1179652
  67.8 1.6 copy-start.3
  67.9 1.7 copy-start.5
  74.4 35.1 %copy-start.1 = (bf16[256,2048]{1,0:T(8,128)(2,1)S(1)}, bf16[256,2048]{1,0:T(8,128)(2,1)}, u32[]{:S(2)}) copy-start(bf16[256,2048]{1,0:T(8,128)(2,1)} %param.15) | copy-start | bytes 3145732
  74.4 130.1 %all-gather.7.cloned.1.call-start = ((), (), s32[]{:S(2)}) async-start(), calls=%async_computation.3 | async-start | bytes 6488064 | tf_op jit(solution)/shard_map/all_gather | solution.py:110
  75.1 222.6 %all-gather.11.cloned.1.call-start = ((), (), s32[]{:S(2)}) async-start(), calls=%async_computation.5 | async-start | bytes 6488064 | tf_op jit(solution)/shard_map/all_gather | solution.py:117
  75.7 314.5 %all-gather.9.cloned.1.call-start = ((), (), s32[]{:S(2)}) async-start(), calls=%async_computation.4 | async-start | bytes 6488064 | tf_op jit(solution)/shard_map/all_gather | solution.py:113
  76.3 128.2 %copy-start.7 = (f32[2048]{0:T(1024)S(1)}, f32[2048]{0:T(1024)}, u32[]{:S(2)}) copy-start(f32[2048]{0:T(1024)} %param.26) | copy-start | bytes 24580
  76.3 346.7 %reduce-scatter.2.cloned.1.call-start = ((), (), s32[]{:S(2)}) async-start(), calls=%async_computation.6 | async-start | bytes 1310720 | tf_op jit(solution)/shard_map/reduce_scatter | solution.py:119
Sparse Core Ops, SparseCore 0:
  9.7 52.4 all-gather.4
  74.5 34.8 all-reduce.1
  111.6 92.7 all-gather.6
  206.3 91.2 all-gather.10
  299.7 90.4 all-gather.8
  400.0 22.9 reduce-scatter.1
where the time goes:
time: 432 us
  waiting for transfers between devices  345 us (80%)
  blocking collectives  32.9 us (8%)
  matrix products  27.9 us (6%)
  between operations  13.6 us (3%)
  other arithmetic  11.4 us (3%)
    all_gather x1, waiting for transfers between devices, shards(): lax.all_gather(w_up, 'sp', axis=0, tiled=True)  92.6 us
    all_gather x1, waiting for transfers between devices, shards(): lax.all_gather(w_gate, 'sp', axis=0, tiled=True)  92.1 us
    all_gather x1, waiting for transfers between devices, shards(): lax.all_gather(w_down, 'sp', axis=1, tiled=True)  87.3 us
    psum x1, waiting for transfers between devices, shards(): lax.psum(partial_out.astype(jnp.bfloat16), 'tp').astype(jnp.float32)  32.9 us
    all_gather x1, blocking collectives, shards(): rot_piece = lax.all_gather(key_rot, 'sp', axis=0, tiled=True)  32.9 us
    reduce_scatter x1, waiting for transfers between devices, shards(): lax.psum_scatter(terms.astype(jnp.bfloat16), 'tp', scatter_dimension=0, t...  23.1 us
    all_gather x1, waiting for transfers between devices, shards(): latent = lax.all_gather(kv_norm, 'sp', axis=0, tiled=True)  15.4 us
    dot_general x1, matrix products, shards(): jnp.dot(hidden, lax.all_gather(w_down, 'sp', axis=1, tiled=True), preferr...  9.6 us
  transfers between devices with their start and end apart: 6, of which 6 were waited for; matrix products, arithmetic and copies ran while one was open for 3% of the time, Pallas kernels for 0%

commit v1 on v0

--- a/solution.py
+++ b/solution.py
@@ -81,8 +81,11 @@
         jnp.zeros((heads_dev, tok), jnp.float32),
         jnp.zeros((tok, heads_dev, VDIM), jnp.float32),
     )
-    latent = lax.all_gather(kv_norm, "sp", axis=0, tiled=True)
-    rot_piece = lax.all_gather(key_rot, "sp", axis=0, tiled=True)
+    latent, rot_piece = jnp.split(
+        lax.all_gather(jnp.concatenate([kv_norm, key_rot], axis=1), "sp", axis=0, tiled=True),
+        [kv_norm.shape[1]],
+        axis=1,
+    )
     count = latent.shape[0]
     k_piece = (
         jnp.dot(latent, w_key_plain, preferred_element_type=jnp.float32)

time: 432 us -> 436 us (level)
  waiting for transfers between devices: 345 us -> 382 us
  blocking collectives: 32.9 us -> 0 us
    all_gather x1, waiting for transfers between devices: 15.4 us -> 53.1 us  [shards(): lax.all_gather(jnp.concatenate([kv_norm, key_rot], axis=1), 'sp', axis=0,...]
    all_gather x1 -> x0, blocking collectives: 32.9 us -> none  [shards(): rot_piece = lax.all_gather(key_rot, 'sp', axis=0, tiled=True)]
where the time goes in v1:
time: 436 us
  waiting for transfers between devices  382 us (88%)
  matrix products  28.9 us (7%)
  between operations  13.6 us (3%)
  other arithmetic  9.1 us (2%)
    all_gather x1, waiting for transfers between devices, shards(): lax.all_gather(w_up, 'sp', axis=0, tiled=True)  92.6 us
    all_gather x1, waiting for transfers between devices, shards(): lax.all_gather(w_gate, 'sp', axis=0, tiled=True)  92.1 us
    all_gather x1, waiting for transfers between devices, shards(): lax.all_gather(w_down, 'sp', axis=1, tiled=True)  87.3 us
    all_gather x1, waiting for transfers between devices, shards(): lax.all_gather(jnp.concatenate([kv_norm, key_rot], axis=1), 'sp', axis=0,...  53.1 us
    psum x1, waiting for transfers between devices, shards(): lax.psum(partial_out.astype(jnp.bfloat16), 'tp').astype(jnp.float32)  32.5 us
    reduce_scatter x1, waiting for transfers between devices, shards(): lax.psum_scatter(terms.astype(jnp.bfloat16), 'tp', scatter_dimension=0, t...  23.1 us
    dot_general x1, matrix products, shards(): jnp.dot(hidden, lax.all_gather(w_down, 'sp', axis=1, tiled=True), preferr...  9.61 us
  transfers between devices with their start and end apart: 6, of which 6 were waited for; matrix products, arithmetic and copies ran while one was open for 3% of the time, Pallas kernels for 0%

profile of v1, /device:TPU:0, one launch (start us, length us, event | category | flops | bytes accessed | tf_op | source)
XLA Modules:
  0.0 436.0 jit_solution(15678040587162184473)
XLA Ops:
  6.5 0.0 copy-start
  6.5 0.0 all-gather.5.cloned.1.call-start
  6.6 0.9 convert_element_type.66
  7.5 1.1 copy.16
  8.6 0.1 fusion.22
  8.7 0.8 fusion.24
  9.5 0.2 multiply_cosine_fusion
  9.7 0.0 copy-start.4
  9.7 0.7 pad_maximum_fusion
  10.5 0.0 all-gather.5.cloned.1.call-update
  10.5 0.0 all-reduce.2.cloned.1.call-start
  10.6 0.0 copy-done.2
  10.6 0.2 fusion.19
  10.7 0.0 copy-done.7
  10.7 1.5 fusion.12
  12.3 1.4 fusion.31
  13.7 53.1 %all-gather.5.cloned.1.call-done = bf16[2048,576]{0,1:T(8,128)(2,1)} async-done(((bf16[256,576]{0,1:T(8,128)(2,1)}), bf16[2048,576]{0,1:T(8,128)(2,1)}) %all-gather.5.cloned.1.call-update) | async-done | bytes 2359312 | tf_op jit(solution)/shard_map/all_gather | solution.py:85
  66.9 0.0 copy-done.4
  66.9 2.9 convolution_convert_fusion
  69.8 0.0 copy-start.3
  69.8 1.2 fusion.25
  71.0 0.4 copy-done.3
  71.4 1.4 fusion.37
  72.9 0.0 copy-start.5
  72.9 1.3 fusion.1
  74.2 1.3 convolution_convert_fusion.1
  75.5 1.8 fusion.16
  77.3 0.0 copy-done
  77.3 1.7 convolution_convert_fusion.2
  79.0 0.0 all-reduce.2.cloned.1.call-update
  79.1 0.0 all-gather.7.cloned.1.call-start
  79.1 0.7 all-gather.7.cloned.1.call-update
  79.8 0.0 all-gather.11.cloned.1.call-start
  79.8 0.5 all-gather.11.cloned.1.call-update
  80.4 0.0 all-gather.9.cloned.1.call-start
  80.4 0.5 all-gather.9.cloned.1.call-update
  81.0 0.0 copy-start.6
  81.0 0.2 reduce-scatter.2.cloned.1.call-start
  81.2 32.5 %all-reduce.2.cloned.1.call-done = bf16[256,2048]{1,0:T(8,128)(2,1)} async-done(((bf16[256,2048]{1,0:T(8,128)(2,1)}), bf16[256,2048]{1,0:T(8,128)(2,1)}) %all-reduce.2.cloned.1.call-update) | async-done | bytes 1048592 | tf_op jit(solution)/shard_map/psum | solution.py:107
  113.7 2.9 convert_add_fusion
  116.6 92.1 %all-gather.7.cloned.1.call-done = bf16[2048,1408]{1,0:T(8,128)(2,1)} async-done(((bf16[256,1408]{1,0:T(8,128)(2,1)}), bf16[2048,1408]{1,0:T(8,128)(2,1)}) %all-gather.7.cloned.1.call-update) | async-done | bytes 5767184 | tf_op jit(solution)/shard_map/all_gather | solution.py:113
  208.7 5.9 %fusion.36 = f32[256,1408]{1,0:T(8,128)} fusion(bf16[2048,1408]{1,0:T(8,128)(2,1)} %all-gather.7.cloned.1.call-done, f32[2048]{0:T(1024)S(1)} %copy-done.6, f32[256]{0:T(256)S(1)} %add_rsqrt_fusion, bf16[256,2048]{1,0:T(8,128)(2,1)} %all-reduce.2.cloned.1.call-done, bf16[256,2048]{1,0:T(8,128)(2,1)S(1)} %copy-done.1), kind=kOutput, calls=%fused_computation.57 | convolution fusion | flops 1479540736 | bytes 9315328 | tf_op jit(solution)/shard_map/dot_general | solution.py:112
  214.6 87.3 %all-gather.11.cloned.1.call-done = bf16[1408,2048]{1,0:T(8,128)(2,1)} async-done(((bf16[1408,256]{1,0:T(8,128)(2,1)}), bf16[1408,2048]{1,0:T(8,128)(2,1)}) %all-gather.11.cloned.1.call-update) | async-done | bytes 5767184 | tf_op jit(solution)/shard_map/all_gather | solution.py:120
  301.9 92.6 %all-gather.9.cloned.1.call-done = bf16[2048,1408]{1,0:T(8,128)(2,1)} async-done(((bf16[256,1408]{1,0:T(8,128)(2,1)}), bf16[2048,1408]{1,0:T(8,128)(2,1)}) %all-gather.9.cloned.1.call-update) | async-done | bytes 5767184 | tf_op jit(solution)/shard_map/all_gather | solution.py:116
  394.5 9.6 %convolution_convert_fusion.3 = bf16[256,2048]{1,0:T(8,128)(2,1)} fusion(bf16[1408,2048]{1,0:T(8,128)(2,1)} %all-gather.11.cloned.1.call-done, bf16[2048,1408]{1,0:T(8,128)(2,1)} %all-gather.9.cloned.1.call-done, f32[256,1408]{1,0:T(8,128)} %fusion.36, f32[2048]{0:T(1024)S(1)} %copy-done.6, f32[256]{0:T(256)S(1)} %add_rsqrt_fusion, ...), kind=kOutput, calls=%fused_computation.12 | convolution fusion | flops 2958622720 | bytes 16131072 | tf_op jit(solution)/shard_map/dot_general | solution.py:119
  404.1 0.0 reduce-scatter.2.cloned.1.call-update
  404.1 23.1 %reduce-scatter.2.cloned.1.call-done = bf16[64,2048]{1,0:T(8,128)(2,1)} async-done(((bf16[256,2048]{1,0:T(8,128)(2,1)}), bf16[64,2048]{1,0:T(8,128)(2,1)}) %reduce-scatter.2.cloned.1.call-update) | async-done | bytes 262160 | tf_op jit(solution)/shard_map/reduce_scatter | solution.py:122
  427.3 1.9 add_convert_fusion
  (13 shorter events, 0.1 us)
Async XLA Ops:
  6.5 70.8 %copy-start = (bf16[512,2048]{1,0:T(8,128)(2,1)S(1)}, bf16[512,2048]{1,0:T(8,128)(2,1)}, u32[]{:S(2)}) copy-start(bf16[512,2048]{1,0:T(8,128)(2,1)} %param.25) | copy-start | bytes 6291460
  6.5 4.0 copy-start.2
  6.5 4.2 copy-start.7
  6.5 60.3 %all-gather.5.cloned.1.call-start = ((), (), s32[]{:S(2)}) async-start(), calls=%async_computation.1 | async-start | bytes 2654208 | tf_op jit(solution)/shard_map/all_gather | solution.py:85
  9.7 57.2 %copy-start.4 = (bf16[512,512]{1,0:T(8,128)(2,1)S(1)}, bf16[512,512]{1,0:T(8,128)(2,1)}, u32[]{:S(2)}) copy-start(bf16[512,512]{1,0:T(8,128)(2,1)} %param.23) | copy-start | bytes 1572868
  10.5 103.2 %all-reduce.2.cloned.1.call-start = ((), (), s32[]{:S(2)}) async-start(), calls=%async_computation.2 | async-start | bytes 2097152 | tf_op jit(solution)/shard_map/psum | solution.py:107
  69.8 1.7 copy-start.3
  72.9 1.3 copy-start.5
  79.0 34.6 %copy-start.1 = (bf16[256,2048]{1,0:T(8,128)(2,1)S(1)}, bf16[256,2048]{1,0:T(8,128)(2,1)}, u32[]{:S(2)}) copy-start(bf16[256,2048]{1,0:T(8,128)(2,1)} %param.15) | copy-start | bytes 3145732
  79.1 129.6 %all-gather.7.cloned.1.call-start = ((), (), s32[]{:S(2)}) async-start(), calls=%async_computation.3 | async-start | bytes 6488064 | tf_op jit(solution)/shard_map/all_gather | solution.py:113
  79.8 222.1 %all-gather.11.cloned.1.call-start = ((), (), s32[]{:S(2)}) async-start(), calls=%async_computation.5 | async-start | bytes 6488064 | tf_op jit(solution)/shard_map/all_gather | solution.py:120
  80.4 314.1 %all-gather.9.cloned.1.call-start = ((), (), s32[]{:S(2)}) async-start(), calls=%async_computation.4 | async-start | bytes 6488064 | tf_op jit(solution)/shard_map/all_gather | solution.py:116
  81.0 127.7 %copy-start.6 = (f32[2048]{0:T(1024)S(1)}, f32[2048]{0:T(1024)}, u32[]{:S(2)}) copy-start(f32[2048]{0:T(1024)} %param.26) | copy-start | bytes 24580
  81.0 346.3 %reduce-scatter.2.cloned.1.call-start = ((), (), s32[]{:S(2)}) async-start(), calls=%async_computation.6 | async-start | bytes 1310720 | tf_op jit(solution)/shard_map/reduce_scatter | solution.py:122
Sparse Core Ops, SparseCore 0:
  10.6 56.2 all-gather.4
  79.2 34.4 all-reduce.1
  115.9 92.7 all-gather.6
  210.6 91.3 all-gather.10
  304.0 90.4 all-gather.8
  404.2 22.9 reduce-scatter.1
